TPU v7x, 32 devices: a whole 2x2x4 slice. The times are simulated.
32 devices in a mesh: kv: 4 (over y, x), tp: 8 (over z, core).
Axes of the slice: x: 2, y: 2, z: 4, core: 2. Of those that a mesh axis runs over, the one named last changes fastest.
Arguments:
- tokens: bfloat16 [16, 2048], P(None, 'kv'), may hold values from -40 to 40
- lengths: int32 [16], replicated, may hold values from 1 to 4096, 19456 in all
- cache_keys: bfloat16 [16, 4096, 16, 128], P(None, 'kv', 'tp'), may hold values from -200 to 200
- cache_values: bfloat16 [16, 4096, 16, 128], P(None, 'kv', 'tp'), may hold values from -6 to 6
- lambdas: float32 [16], P('tp'), may hold values from 0.3 to 0.8
- head_gain: bfloat16 [128], replicated, may hold values from 0.099609375 to 1.8984375
- attn_gain: bfloat16 [2048], P('kv'), may hold values from 0.099609375 to 1.8984375
- w_query: bfloat16 [2048, 2048], P('kv', 'tp'), may hold values from -0.125 to 0.125
- w_key: bfloat16 [2048, 2048], P('kv', 'tp'), may hold values from -0.5 to 0.5
- w_value: bfloat16 [2048, 2048], P('kv', 'tp'), may hold values from -0.125 to 0.125
- w_out: bfloat16 [2048, 2048], P('tp', 'kv'), may hold values from -0.125 to 0.125
- first_gain: bfloat16 [2048], P('kv'), may hold values from 0.099609375 to 1.8984375
- first_gate: bfloat16 [2048, 5632], P('kv', 'tp'), may hold values from -0.125 to 0.125
- first_up: bfloat16 [2048, 5632], P('kv', 'tp'), may hold values from -0.125 to 0.125
- first_down: bfloat16 [5632, 2048], P('tp', 'kv'), may hold values from -0.078125 to 0.078125
- second_gain: bfloat16 [2048], P('kv'), may hold values from 0.099609375 to 1.8984375
- second_gate: bfloat16 [2048, 5632], P('kv', 'tp'), may hold values from -0.125 to 0.125
- second_up: bfloat16 [2048, 5632], P('kv', 'tp'), may hold values from -0.125 to 0.125
- second_down: bfloat16 [5632, 2048], P('tp', 'kv'), may hold values from -0.078125 to 0.078125
Outputs:
- stream_out: bfloat16 [16, 2048], P(None, 'kv')
Inputs may be any that keep to these rules, and one draw needn't show every extreme that they name: `lengths`: one sequence has exactly 4096 live positions.
All inputs are finite; a program needn't handle non-finite values.
Results may differ from a plain program's by a relative error of at most 0.02.
Values may be sent and summed in bfloat16 or wider, within the bound.
A program may use at most 64 MiB of HBM per device.

v0:
```python
import functools

import jax
import jax.numpy as jnp
import numpy as np
from jax import lax
from jax.experimental import pallas as pl
from jax.experimental.pallas import tpu as pltpu
from jax.sharding import PartitionSpec as P

EPSILON = 1e-06
ROTARY_BASE = 10000.0
OUTPUT_KEEP = 0.8
MASKED_SCORE = -1e30
F32 = jnp.float32
BF16 = jnp.bfloat16
MESH = pl.DeviceIdType.MESH
GROUP = 4


def turned(left, right):
    return lax.dot_general(left, right, (((1,), (1,)), ((), ())), preferred_element_type=F32)


def near_first(n):
    return sorted(range(1, n), key=lambda k: (min(k, n - k), k))


def kernel(
    n_kv,
    n_tp,
    width,
    tokens_hbm,
    lengths,
    keys_hbm,
    values_hbm,
    lambdas,
    head_gain,
    attn_gain,
    wq_hbm,
    wk_hbm,
    wv_hbm,
    wo_hbm,
    first_gain,
    fg_hbm,
    fu_hbm,
    fd_hbm,
    second_gain,
    sg_hbm,
    su_hbm,
    sd_hbm,
    inv_freq,
    out_ref,
    tokens,
    keys,
    values,
    wq,
    wk,
    wv,
    wo,
    fg,
    fu,
    fd,
    sg,
    su,
    sd,
    mix1,
    mix2,
    down1,
    down2,
    proj,
    qnew,
    knew,
    vnew,
    part,
    qrows,
    load_sem,
    kv_send,
    kv_recv,
    tp_send,
    tp_recv,
):
    me_kv = lax.axis_index("kv")
    me_tp = lax.axis_index("tp")
    seqs, cols = tokens.shape
    units = fg.shape[0]
    pad = mix1.shape[-1]
    heads = wq.shape[1] // 128
    rows = 2 * heads

    loads = {}
    for number, (name, source, target) in enumerate(
        (
            ("tokens", tokens_hbm, tokens),
            ("fg", fg_hbm, fg),
            ("fu", fu_hbm, fu),
            ("fd", fd_hbm, fd),
            ("wq", wq_hbm, wq),
            ("wk", wk_hbm, wk),
            ("wv", wv_hbm, wv),
            ("keys", keys_hbm, keys),
            ("values", values_hbm, values),
            ("wo", wo_hbm, wo),
            ("sg", sg_hbm, sg),
            ("su", su_hbm, su),
            ("sd", sd_hbm, sd),
        )
    ):
        loads[name] = pltpu.make_async_copy(source, target, load_sem.at[number])
        if number < 4:
            loads[name].start()

    barrier = pltpu.get_barrier_semaphore()
    for k in near_first(n_kv):
        pl.semaphore_signal(
            barrier, inc=1, device_id={"kv": lax.rem(me_kv + k, n_kv)}, device_id_type=MESH
        )
    for k in near_first(n_tp):
        pl.semaphore_signal(
            barrier, inc=1, device_id={"tp": lax.rem(me_tp + k, n_tp)}, device_id_type=MESH
        )

    started = []

    def send(slot, axis, number):
        if axis == "kv":
            n, me, send_sem, recv_sem = n_kv, me_kv, kv_send, kv_recv
        else:
            n, me, send_sem, recv_sem = n_tp, me_tp, tp_send, tp_recv
        copies = []
        for k in near_first(n):
            copy = pltpu.make_async_remote_copy(
                src_ref=slot(me),
                dst_ref=slot(me),
                send_sem=send_sem.at[number, k - 1],
                recv_sem=recv_sem.at[number, k - 1],
                device_id={axis: lax.rem(me + k, n)},
                device_id_type=MESH,
            )
            copy.start()
            copies.append(copy)
        started.extend(copies)
        return copies

    def receive(copies):
        for copy in copies:
            copy.wait_recv()

    def scaled_of(stream_f, gain):
        scaled = (stream_f * gain[...].astype(F32)).astype(BF16)
        return scaled, jnp.sum(stream_f * stream_f, axis=1, keepdims=True)

    def half_step(stream_f, gain, gate, up, downw, names, mix, down, number, ready, after):
        scaled, square = scaled_of(stream_f, gain)
        high = square.astype(BF16)
        low = (square - high.astype(F32)).astype(BF16)
        loads[names[0]].wait()
        mix[me_kv, 0, :, :units] = turned(scaled, gate[...]).astype(
            BF16
        )
        mix[me_kv, 0, :, units:] = jnp.broadcast_to(high, (seqs, pad - units))
        ready()
        sent = send(lambda i: mix.at[i, 0], "kv", number)
        loads[names[1]].wait()
        mix[me_kv, 1, :, :units] = turned(scaled, up[...]).astype(BF16)
        mix[me_kv, 1, :, units:] = jnp.broadcast_to(low, (seqs, pad - units))
        sent = sent + send(lambda i: mix.at[i, 1], "kv", number + 1)
        after()
        loads[names[2]].wait()
        receive(sent)
        gate_sum = mix[0, 0].astype(F32)
        up_sum = mix[0, 1].astype(F32)
        for i in range(1, n_kv):
            gate_sum = gate_sum + mix[i, 0].astype(F32)
            up_sum = up_sum + mix[i, 1].astype(F32)
        total = gate_sum[:, units : units + 1] + up_sum[:, units : units + 1]
        row_scale = lax.rsqrt(total / width + EPSILON)
        gated = row_scale * gate_sum[:, :units]
        hidden = (gated * jax.nn.sigmoid(gated) * (row_scale * up_sum[:, :units])).astype(BF16)
        return reduced(jnp.dot(hidden, downw[...], preferred_element_type=F32), down, number // 2)

    def reduced(partial, buffer, number):
        buffer[me_tp] = partial.astype(buffer.dtype)
        receive(send(lambda i: buffer.at[i], "tp", number))
        total = buffer[0].astype(F32)
        for i in range(1, n_tp):
            total = total + buffer[i].astype(F32)
        return total

    def ready():
        pl.semaphore_wait(barrier, n_kv + n_tp - 2)

    def load_rest():
        for name in list(loads)[4:]:
            loads[name].start()

    loads["tokens"].wait()
    stream = tokens[...].astype(F32)
    mixed_sum = half_step(
        stream, first_gain, fg, fu, fd, ("fg", "fu", "fd"), mix1, down1, 0, ready, load_rest
    )
    first = (stream + 0.5 * mixed_sum).astype(BF16).astype(F32)

    scaled, square = scaled_of(first, attn_gain)
    loads["wq"].wait()
    span = heads * 128
    qnew[me_kv, :, :span] = jnp.dot(scaled, wq[...], preferred_element_type=F32)
    qnew[me_kv, :, span:] = jnp.broadcast_to(square, (seqs, 128))
    q_sent = send(lambda i: qnew.at[i], "kv", 4)
    loads["wk"].wait()
    knew[me_kv] = jnp.dot(scaled, wk[...], preferred_element_type=F32)
    kv_sent = send(lambda i: knew.at[i], "kv", 5)
    loads["wv"].wait()
    vnew[me_kv] = jnp.dot(scaled, wv[...], preferred_element_type=F32).astype(BF16)
    kv_sent = kv_sent + send(lambda i: vnew.at[i], "kv", 6)

    lane = lax.broadcasted_iota(jnp.int32, (seqs, 128), 1)
    row = lax.broadcasted_iota(jnp.int32, (seqs, 128), 0)
    position = jnp.zeros((seqs, 128), jnp.int32)
    for b in range(seqs):
        position = jnp.where(row == b, lengths[b], position)
    angles = position.astype(F32) * inv_freq[...]
    cosine = jnp.cos(angles)
    sine = jnp.sin(angles)
    lower = lax.rem(lane, 64) < 32
    sine = jnp.where(lower, -sine, sine)
    left_half = lane < 64

    def rotated(x):
        other = jnp.where(lower, pltpu.roll(x, 96, 1), pltpu.roll(x, 32, 1))
        return (x * cosine + other * sine).astype(BF16).astype(F32)

    places = keys.shape[1] // heads
    shape = (8, keys.shape[1])
    column = lax.broadcasted_iota(jnp.int32, shape, 1)
    query_row = lax.broadcasted_iota(jnp.int32, shape, 0)
    spot = me_kv * places + lax.div(column, heads)
    spot = jnp.where(lax.rem(column, heads) == lax.div(query_row, 2), spot, 1 << 30)

    qrows[...] = jnp.zeros_like(qrows)
    receive(q_sent)
    sums = qnew[0]
    for i in range(1, n_kv):
        sums = sums + qnew[i]
    row_scale = lax.rsqrt(sums[:, span : span + 1] / width + EPSILON)
    queries = []
    for h in range(heads):
        query = rotated(row_scale * sums[:, h * 128 : (h + 1) * 128])
        queries.append(query)
        for c in range(2):
            half = left_half if c == 0 else jnp.logical_not(left_half)
            qrows[:, 2 * h + c, :] = jnp.where(half, query, 0.0)

    loads["keys"].wait()
    loads["values"].wait()
    lane8 = lax.broadcasted_iota(jnp.int32, (8, 128), 1)

    part_sent = []
    for step in range(seqs // GROUP):
        for b in range(step * GROUP, (step + 1) * GROUP):
            scores = (
                turned(qrows[b].astype(BF16), keys[b]) * 0.125
            )
            live = spot < lengths[b]
            scores = jnp.where(live, scores, MASKED_SCORE)
            peak = jnp.max(scores, axis=1, keepdims=True)
            weights = jnp.where(live, jnp.exp(scores - peak), 0.0)
            total = jnp.sum(weights, axis=1, keepdims=True)
            summed = jnp.dot(weights.astype(BF16), values[b], preferred_element_type=F32)
            stats = jnp.where(lane8 < 64, peak, total)
            part[me_kv, b, :rows, :] = summed[:rows]
            part[me_kv, b, rows : 2 * rows, :] = stats[:rows]
        group = pl.ds(step * GROUP, GROUP)
        part_sent = part_sent + send(lambda i: part.at[i, group], "kv", 7 + step)

    receive(kv_sent)
    key_sum = knew[0]
    for i in range(1, n_kv):
        key_sum = key_sum + knew[i]
    own = []
    for h in range(heads):
        fresh = rotated(row_scale * key_sum[:, h * 128 : (h + 1) * 128])
        product = queries[h] * fresh
        for c in range(2):
            half = left_half if c == 0 else jnp.logical_not(left_half)
            own.append(jnp.sum(jnp.where(half, product, 0.0), axis=1, keepdims=True) * 0.125)
    value_sum = vnew[0].astype(F32)
    for i in range(1, n_kv):
        value_sum = value_sum + vnew[i].astype(F32)
    fresh_value = (row_scale * value_sum).astype(BF16).astype(F32)
    loads["wo"].wait()
    receive(part_sent)
    projected = None
    for h in range(heads):
        maps = []
        for c in range(2):
            r = 2 * h + c
            stats = [part[i, :, rows + r, :] for i in range(n_kv)]
            peaks = [s[:, 0:1] for s in stats]
            top = own[r]
            for peak in peaks:
                top = jnp.maximum(top, peak)
            fresh_weight = jnp.exp(own[r] - top)
            below = fresh_weight
            above = fresh_weight * fresh_value[:, h * 128 : (h + 1) * 128]
            for i in range(n_kv):
                share = jnp.exp(peaks[i] - top)
                below = below + stats[i][:, 64:65] * share
                above = above + part[i, :, r, :] * share
            maps.append(above / below)
        head = maps[0] - lambdas[h] * maps[1]
        norm = lax.rsqrt(jnp.mean(head * head, axis=1, keepdims=True) + EPSILON)
        normed = (head * norm * head_gain[...].astype(F32) * OUTPUT_KEEP).astype(BF16)
        term = jnp.dot(normed, wo[h * 128 : (h + 1) * 128, :], preferred_element_type=F32)
        projected = term if projected is None else projected + term
    second = (first + reduced(projected, proj, 2)).astype(BF16).astype(F32)

    nothing = (lambda: None, lambda: None)
    mixed_sum = half_step(
        second, second_gain, sg, su, sd, ("sg", "su", "sd"), mix2, down2, 2, *nothing
    )
    out_ref[...] = (second + 0.5 * mixed_sum).astype(BF16)
    for copy in started:
        copy.wait_send()


def local(n_kv, n_tp, *args):
    (
        tokens,
        lengths,
        cache_keys,
        cache_values,
        lambdas,
        head_gain,
        attn_gain,
        w_query,
        w_key,
        w_value,
        w_out,
        first_gain,
        first_gate,
        first_up,
        first_down,
        second_gain,
        second_gate,
        second_up,
        second_down,
    ) = args
    seqs, cols = tokens.shape
    places, heads, wide = cache_keys.shape[1:]
    flat = (seqs, places * heads, wide)
    keys = cache_keys.reshape(flat)
    values = cache_values.reshape(flat)
    first_gate, first_up, second_gate, second_up = (
        a.T for a in (first_gate, first_up, second_gate, second_up)
    )
    units = first_gate.shape[0]
    pad = (units // 128 + 1) * 128
    span = heads * 128
    half = np.float32(ROTARY_BASE) ** (-np.arange(32, dtype=np.float32) / np.float32(32))
    inv_freq = jnp.asarray(np.tile(half.astype(np.float32), 4)[None, :])
    hbm = pl.BlockSpec(memory_space=pl.ANY)
    vmem = pl.BlockSpec(memory_space=pltpu.VMEM)
    smem = pl.BlockSpec(memory_space=pltpu.SMEM)
    stay = [tokens, keys, values, w_query, w_key, w_value, w_out]
    stay += [first_gate, first_up, first_down, second_gate, second_up, second_down]
    dma = pltpu.SemaphoreType.DMA
    return pl.pallas_call(
        functools.partial(kernel, n_kv, n_tp, cols * n_kv),
        out_shape=jax.ShapeDtypeStruct((seqs, cols), BF16),
        in_specs=[
            hbm,
            smem,
            hbm,
            hbm,
            smem,
            vmem,
            vmem,
            hbm,
            hbm,
            hbm,
            hbm,
            vmem,
            hbm,
            hbm,
            hbm,
            vmem,
            hbm,
            hbm,
            hbm,
            vmem,
        ],
        out_specs=vmem,
        scratch_shapes=[pltpu.VMEM(a.shape, a.dtype) for a in stay]
        + [
            pltpu.VMEM((n_kv, 2, seqs, pad), BF16),
            pltpu.VMEM((n_kv, 2, seqs, pad), BF16),
            pltpu.VMEM((n_tp, seqs, cols), BF16),
            pltpu.VMEM((n_tp, seqs, cols), BF16),
            pltpu.VMEM((n_tp, seqs, cols), BF16),
            pltpu.VMEM((n_kv, seqs, span + 128), F32),
            pltpu.VMEM((n_kv, seqs, span), F32),
            pltpu.VMEM((n_kv, seqs, span), BF16),
            pltpu.VMEM((n_kv, seqs, 8, 128), F32),
            pltpu.VMEM((seqs, 8, 128), F32),
            dma((len(stay),)),
            dma((7 + seqs // GROUP, n_kv - 1)),
            dma((7 + seqs // GROUP, n_kv - 1)),
            dma((3, n_tp - 1)),
            dma((3, n_tp - 1)),
        ],
        compiler_params=pltpu.CompilerParams(
            collective_id=0, has_side_effects=True, vmem_limit_bytes=56 * 1024 * 1024
        ),
    )(
        tokens,
        lengths,
        keys,
        values,
        lambdas,
        head_gain,
        attn_gain,
        w_query,
        w_key,
        w_value,
        w_out,
        first_gain,
        first_gate,
        first_up,
        first_down,
        second_gain,
        second_gate,
        second_up,
        second_down,
        inv_freq,
    )


def solution(mesh):
    return jax.shard_map(
        functools.partial(local, mesh.shape["kv"], mesh.shape["tp"]),
        mesh=mesh,
        in_specs=(
            P(None, "kv"),
            P(),
            P(None, "kv", "tp", None),
            P(None, "kv", "tp", None),
            P("tp"),
            P(),
            P("kv"),
            P("kv", "tp"),
            P("kv", "tp"),
            P("kv", "tp"),
            P("tp", "kv"),
            P("kv"),
            P("kv", "tp"),
            P("kv", "tp"),
            P("tp", "kv"),
            P("kv"),
            P("kv", "tp"),
            P("kv", "tp"),
            P("tp", "kv"),
        ),
        out_specs=P(None, "kv"),
        check_vma=False,
    )
```

profile of v0, /device:TPU:0, one launch (start us, length us, event | category | flops | bytes accessed | tf_op | source)
XLA Modules:
  0.0 45.5 jit_solution(2284406416241132269)
XLA Ops:
  0.0 44.1 %shard_map.190 = bf16[16,512]{1,0:T(8,128)(2,1)} custom-call(bf16[16,512]{1,0:T(8,128)(2,1)} %tokens_hbm.1, s32[16]{0:T(128)} %lengths.1, bf16[16,2048,128]{2,1,0:T(8,128)(2,1)} %bitcast.6, bf16[16,2048,128]{2,1,0:T(8,128)(2,1)} %bitcast.7, f32[2]{0:T(128)} %lambdas.1, bf16[128]{0:T(256)(128)(2,1)} %head_gain.1, bf16[512]{0:T(512)(128)(2,1)} %attn_gain.1, ...), custom_call_target="tpu_custom_call" | custom-call | tf_op jit(solution)/shard_map/pallas_call | solution.py:368
  44.1 1.3 %copy.22 = bf16[16,512]{1,0:T(8,128)(2,1)} copy(bf16[16,512]{1,0:T(8,128)(2,1)} %shard_map.190) | data formatting | bytes 32768
where the time goes:
time: 45.8 us; the launch traced here: 45.5 us
  Pallas kernels  44.1 us (96%)
  local copies, waits for them, and re-layouts  1.32 us (3%)
    pallas_call x1, Pallas kernels, local(): pl.pallas_call(functools.partial(kernel, n_kv, n_tp, cols * n_kv), out_sh...  44.1 us
    unnamed x1, local copies, waits for them, and re-layouts  1.32 us

commit v1 on v0

v1 whole, which is shorter than its diff:
```python
import functools

import jax
import jax.numpy as jnp
import numpy as np
from jax import lax
from jax.experimental import pallas as pl
from jax.experimental.pallas import tpu as pltpu
from jax.sharding import PartitionSpec as P

EPSILON = 1e-06
ROTARY_BASE = 10000.0
OUTPUT_KEEP = 0.8
MASKED_SCORE = -1e30
F32 = jnp.float32
BF16 = jnp.bfloat16
MESH = pl.DeviceIdType.MESH
AHEAD = 2


def turned(left, right):
    return lax.dot_general(left, right, (((1,), (1,)), ((), ())), preferred_element_type=F32)


def partners(n):
    return range(n - 1, 0, -1)


def flipped(me, mask):
    other = me
    bit = 1
    while bit <= mask:
        if mask & bit:
            other = other + bit * (1 - 2 * lax.rem(lax.div(me, bit), 2))
        bit *= 2
    return other


def kernel(
    n_kv,
    n_tp,
    width,
    tokens_hbm,
    lengths_hbm,
    keys_hbm,
    values_hbm,
    lambdas_hbm,
    head_gain_hbm,
    attn_gain_hbm,
    wq_hbm,
    wk_hbm,
    wv_hbm,
    wo_hbm,
    first_gain_hbm,
    fg_hbm,
    fu_hbm,
    fd_hbm,
    second_gain_hbm,
    sg_hbm,
    su_hbm,
    sd_hbm,
    inv_freq_hbm,
    out_ref,
    tokens,
    keys,
    values,
    wq,
    wk,
    wv,
    wo,
    fg,
    fu,
    fd,
    sg,
    su,
    sd,
    head_gain,
    attn_gain,
    first_gain,
    second_gain,
    inv_freq,
    lengths,
    lambdas,
    mix1,
    mix2,
    down1,
    down2,
    proj,
    qnew,
    knew,
    vnew,
    part,
    stat,
    own_part,
    qrows,
    load_sem,
    kv_send,
    kv_recv,
    tp_send,
    tp_recv,
):
    me_kv = lax.axis_index("kv")
    me_tp = lax.axis_index("tp")
    seqs, cols = tokens.shape
    units = fg.shape[0]
    pad = mix1.shape[-1]
    heads = wq.shape[1] // 128
    rows = 2 * heads

    loads = {}
    for number, (name, source, target) in enumerate(
        (
            ("tokens", tokens_hbm, tokens),
            ("first_gain", first_gain_hbm, first_gain),
            ("fg", fg_hbm, fg),
            ("fu", fu_hbm, fu),
            ("fd", fd_hbm, fd),
            ("lengths", lengths_hbm, lengths),
            ("inv_freq", inv_freq_hbm, inv_freq),
            ("attn_gain", attn_gain_hbm, attn_gain),
            ("wq", wq_hbm, wq),
            ("wk", wk_hbm, wk),
            ("wv", wv_hbm, wv),
            ("keys", keys_hbm, keys),
            ("values", values_hbm, values),
            ("lambdas", lambdas_hbm, lambdas),
            ("head_gain", head_gain_hbm, head_gain),
            ("wo", wo_hbm, wo),
            ("second_gain", second_gain_hbm, second_gain),
            ("sg", sg_hbm, sg),
            ("su", su_hbm, su),
            ("sd", sd_hbm, sd),
        )
    ):
        loads[name] = pltpu.make_async_copy(source, target, load_sem.at[number])

    def load(*names):
        for name in names:
            loads[name].start()

    def loaded(*names):
        for name in names:
            loads[name].wait()

    load("tokens", "first_gain", "fg", "fu")
    barrier = pltpu.get_barrier_semaphore()
    kv_ids = {m: {"kv": flipped(me_kv, m)} for m in partners(n_kv)}
    tp_ids = {m: {"tp": flipped(me_tp, m)} for m in partners(n_tp)}
    for ids in (kv_ids, tp_ids):
        for device in ids.values():
            pl.semaphore_signal(barrier, inc=1, device_id=device, device_id_type=MESH)
    load("fd", "lengths", "inv_freq", "attn_gain")

    started = []

    def send(slot, axis, number):
        if axis == "kv":
            ids, me, send_sem, recv_sem = kv_ids, me_kv, kv_send, kv_recv
        else:
            ids, me, send_sem, recv_sem = tp_ids, me_tp, tp_send, tp_recv
        copies = []
        for m, device in ids.items():
            copy = pltpu.make_async_remote_copy(
                src_ref=slot(me),
                dst_ref=slot(me),
                send_sem=send_sem.at[number, m - 1],
                recv_sem=recv_sem.at[number, m - 1],
                device_id=device,
                device_id_type=MESH,
            )
            copy.start()
            copies.append(copy)
        started.extend(copies)
        return copies

    def receive(copies):
        for copy in copies:
            copy.wait_recv()

    def settle(keep=0):
        while len(started) > keep:
            started.pop(0).wait_send()

    def scaled_of(stream_f, gain):
        scaled = (stream_f * gain[...].astype(F32)).astype(BF16)
        return scaled, jnp.sum(stream_f * stream_f, axis=1, keepdims=True)

    def half_step(stream_f, gain, gate, up, downw, names, mix, down, number, ready, after):
        scaled, square = scaled_of(stream_f, gain)
        high = square.astype(BF16)
        low = (square - high.astype(F32)).astype(BF16)
        loaded(names[0])
        mix[me_kv, 0, :, :units] = turned(scaled, gate[...]).astype(BF16)
        mix[me_kv, 0, :, units:] = jnp.broadcast_to(high, (seqs, pad - units))
        ready()
        sent = send(lambda i: mix.at[i, 0], "kv", number)
        loaded(names[1])
        mix[me_kv, 1, :, :units] = turned(scaled, up[...]).astype(BF16)
        mix[me_kv, 1, :, units:] = jnp.broadcast_to(low, (seqs, pad - units))
        sent = sent + send(lambda i: mix.at[i, 1], "kv", number + 1)
        after()
        loaded(names[2])
        settle(keep=len(sent))
        receive(sent)
        gate_sum = mix[0, 0].astype(F32)
        up_sum = mix[0, 1].astype(F32)
        for i in range(1, n_kv):
            gate_sum = gate_sum + mix[i, 0].astype(F32)
            up_sum = up_sum + mix[i, 1].astype(F32)
        total = gate_sum[:, units : units + 1] + up_sum[:, units : units + 1]
        row_scale = lax.rsqrt(total / width + EPSILON)
        gated = row_scale * gate_sum[:, :units]
        hidden = (gated * jax.nn.sigmoid(gated) * (row_scale * up_sum[:, :units])).astype(BF16)
        return reduced(jnp.dot(hidden, downw[...], preferred_element_type=F32), down, number // 2)

    def reduced(partial, buffer, number):
        buffer[me_tp] = partial.astype(buffer.dtype)
        sent = send(lambda i: buffer.at[i], "tp", number)
        settle(keep=len(sent))
        receive(sent)
        total = buffer[0].astype(F32)
        for i in range(1, n_tp):
            total = total + buffer[i].astype(F32)
        return total

    def ready():
        pl.semaphore_wait(barrier, n_kv + n_tp - 2)

    def load_rest():
        load("wq", "wk", "wv", "keys", "values", "lambdas", "head_gain", "wo")
        load("second_gain", "sg", "su", "sd")

    loaded("tokens", "first_gain")
    stream = tokens[...].astype(F32)
    mixed_sum = half_step(
        stream, first_gain, fg, fu, fd, ("fg", "fu", "fd"), mix1, down1, 0, ready, load_rest
    )
    first = (stream + 0.5 * mixed_sum).astype(BF16).astype(F32)

    loaded("attn_gain", "wq")
    scaled, square = scaled_of(first, attn_gain)
    span = heads * 128
    qnew[me_kv, :, :span] = jnp.dot(scaled, wq[...], preferred_element_type=F32)
    qnew[me_kv, :, span:] = jnp.broadcast_to(square, (seqs, 128))
    q_sent = send(lambda i: qnew.at[i], "kv", 4)
    loaded("wk")
    knew[me_kv] = jnp.dot(scaled, wk[...], preferred_element_type=F32)
    kv_sent = send(lambda i: knew.at[i], "kv", 5)
    loaded("wv")
    vnew[me_kv] = jnp.dot(scaled, wv[...], preferred_element_type=F32).astype(BF16)
    kv_sent = kv_sent + send(lambda i: vnew.at[i], "kv", 6)
    settle(keep=len(q_sent) + len(kv_sent))

    loaded("lengths", "inv_freq")
    lane = lax.broadcasted_iota(jnp.int32, (seqs, 128), 1)
    row = lax.broadcasted_iota(jnp.int32, (seqs, 128), 0)
    position = jnp.zeros((seqs, 128), jnp.int32)
    for b in range(seqs):
        position = jnp.where(row == b, lengths[b], position)
    angles = position.astype(F32) * inv_freq[...]
    cosine = jnp.cos(angles)
    sine = jnp.sin(angles)
    lower = lax.rem(lane, 64) < 32
    sine = jnp.where(lower, -sine, sine)
    left_half = lane < 64

    def rotated(x):
        other = jnp.where(lower, pltpu.roll(x, 96, 1), pltpu.roll(x, 32, 1))
        return (x * cosine + other * sine).astype(BF16).astype(F32)

    places = keys.shape[1] // heads
    shape = (8, keys.shape[1])
    column = lax.broadcasted_iota(jnp.int32, shape, 1)
    query_row = lax.broadcasted_iota(jnp.int32, shape, 0)
    spot = me_kv * places + lax.div(column, heads)
    spot = jnp.where(lax.rem(column, heads) == lax.div(query_row, 2), spot, 1 << 30)

    qrows[...] = jnp.zeros_like(qrows)
    loaded("keys", "values")
    receive(q_sent)
    sums = qnew[0]
    for i in range(1, n_kv):
        sums = sums + qnew[i]
    row_scale = lax.rsqrt(sums[:, span : span + 1] / width + EPSILON)
    queries = []
    for h in range(heads):
        query = rotated(row_scale * sums[:, h * 128 : (h + 1) * 128])
        queries.append(query)
        for c in range(2):
            half = left_half if c == 0 else jnp.logical_not(left_half)
            qrows[:, 2 * h + c, :] = jnp.where(half, query * 0.125, 0.0)

    scores = {}
    for step in range(seqs + AHEAD):
        if step < seqs:
            scores[step] = turned(qrows[step].astype(BF16), keys[step])
        b = step - AHEAD
        if b < 0:
            continue
        masked = jnp.where(spot < lengths[b], scores.pop(b), MASKED_SCORE)
        peak = jnp.max(masked, axis=1, keepdims=True)
        weights = jnp.exp(masked - jnp.maximum(peak, 0.5 * MASKED_SCORE))
        total = jnp.sum(weights, axis=1, keepdims=True)
        summed = jnp.dot(weights.astype(BF16), values[b], preferred_element_type=F32)
        own_part[0:rows, b, :] = summed[:rows]
        own_part[rows : 2 * rows, b, :] = jnp.broadcast_to(peak, (8, 128))[:rows]
        own_part[2 * rows : 3 * rows, b, :] = jnp.broadcast_to(total, (8, 128))[:rows]
    compact = jnp.zeros((seqs, 128), F32)
    for r in range(rows):
        compact = jnp.where(lane == r, own_part[rows + r], compact)
        compact = jnp.where(lane == 64 + r, own_part[2 * rows + r], compact)
    stat[me_kv] = compact
    stat_sent = send(lambda i: stat.at[i], "kv", 7)
    part[me_kv] = own_part[0:rows].astype(BF16)
    part_sent = send(lambda i: part.at[i], "kv", 8)
    settle(keep=len(stat_sent) + len(part_sent))

    receive(kv_sent)
    key_sum = knew[0]
    for i in range(1, n_kv):
        key_sum = key_sum + knew[i]
    own = jnp.zeros((seqs, 128), F32)
    for h in range(heads):
        fresh = rotated(row_scale * key_sum[:, h * 128 : (h + 1) * 128])
        product = queries[h] * fresh
        for c in range(2):
            half = left_half if c == 0 else jnp.logical_not(left_half)
            score = jnp.sum(jnp.where(half, product, 0.0), axis=1, keepdims=True) * 0.125
            own = jnp.where(lane == 2 * h + c, score, own)
    value_sum = vnew[0].astype(F32)
    for i in range(1, n_kv):
        value_sum = value_sum + vnew[i].astype(F32)
    fresh_value = (row_scale * value_sum).astype(BF16).astype(F32)
    loaded("wo", "lambdas", "head_gain")
    gain_out = head_gain[...].astype(F32) * OUTPUT_KEEP
    receive(stat_sent)
    stats = [stat[i] for i in range(n_kv)]
    top = own
    for s in stats:
        top = jnp.maximum(top, s)
    fresh_weight = jnp.exp(own - top)
    shares = [jnp.exp(s - top) for s in stats]
    below = fresh_weight
    for s, share in zip(stats, shares):
        below = below + pltpu.roll(s, 64, 1) * share
    fresh_weight = fresh_weight / below
    shares = [share / below for share in shares]
    receive(part_sent)
    normed = []
    for h in range(heads):
        maps = []
        for c in range(2):
            r = 2 * h + c
            above = fresh_weight[:, r : r + 1] * fresh_value[:, h * 128 : (h + 1) * 128]
            for i in range(n_kv):
                above = above + shares[i][:, r : r + 1] * part[i, r].astype(F32)
            maps.append(above)
        head = maps[0] - lambdas[h] * maps[1]
        norm = lax.rsqrt(jnp.mean(head * head, axis=1, keepdims=True) + EPSILON)
        normed.append((head * norm * gain_out).astype(BF16))
    projected = jnp.dot(
        jnp.concatenate(normed, axis=1), wo[...], preferred_element_type=F32
    )
    second = (first + reduced(projected, proj, 2)).astype(BF16).astype(F32)

    nothing = (lambda: None, lambda: None)
    loaded("second_gain")
    mixed_sum = half_step(
        second, second_gain, sg, su, sd, ("sg", "su", "sd"), mix2, down2, 2, *nothing
    )
    out_ref[...] = (second + 0.5 * mixed_sum).astype(BF16)
    settle()


def local(n_kv, n_tp, *args):
    (
        tokens,
        lengths,
        cache_keys,
        cache_values,
        lambdas,
        head_gain,
        attn_gain,
        w_query,
        w_key,
        w_value,
        w_out,
        first_gain,
        first_gate,
        first_up,
        first_down,
        second_gain,
        second_gate,
        second_up,
        second_down,
    ) = args
    seqs, cols = tokens.shape
    places, heads, wide = cache_keys.shape[1:]
    flat = (seqs, places * heads, wide)
    keys = cache_keys.reshape(flat)
    values = cache_values.reshape(flat)
    first_gate, first_up, second_gate, second_up = (
        a.T for a in (first_gate, first_up, second_gate, second_up)
    )
    units = first_gate.shape[0]
    pad = (units // 128 + 1) * 128
    span = heads * 128
    half = np.float32(ROTARY_BASE) ** (-np.arange(32, dtype=np.float32) / np.float32(32))
    inv_freq = jnp.asarray(np.tile(half.astype(np.float32), 4)[None, :])
    hbm = pl.BlockSpec(memory_space=pl.ANY)
    stay = [tokens, keys, values, w_query, w_key, w_value, w_out]
    stay += [first_gate, first_up, first_down, second_gate, second_up, second_down]
    stay += [head_gain, attn_gain, first_gain, second_gain, inv_freq]
    dma = pltpu.SemaphoreType.DMA
    return pl.pallas_call(
        functools.partial(kernel, n_kv, n_tp, cols * n_kv),
        out_shape=pltpu.VMEM((seqs, cols), BF16),
        in_specs=[hbm] * 20,
        out_specs=pl.BlockSpec(memory_space=pltpu.VMEM),
        scratch_shapes=[pltpu.VMEM(a.shape, a.dtype) for a in stay]
        + [pltpu.SMEM(a.shape, a.dtype) for a in (lengths, lambdas)]
        + [
            pltpu.VMEM((n_kv, 2, seqs, pad), BF16),
            pltpu.VMEM((n_kv, 2, seqs, pad), BF16),
            pltpu.VMEM((n_tp, seqs, cols), BF16),
            pltpu.VMEM((n_tp, seqs, cols), BF16),
            pltpu.VMEM((n_tp, seqs, cols), BF16),
            pltpu.VMEM((n_kv, seqs, span + 128), F32),
            pltpu.VMEM((n_kv, seqs, span), F32),
            pltpu.VMEM((n_kv, seqs, span), BF16),
            pltpu.VMEM((n_kv, 2 * heads, seqs, 128), BF16),
            pltpu.VMEM((n_kv, seqs, 128), F32),
            pltpu.VMEM((6 * heads, seqs, 128), F32),
            pltpu.VMEM((seqs, 8, 128), F32),
            dma((len(stay) + 2,)),
            dma((9, n_kv - 1)),
            dma((9, n_kv - 1)),
            dma((3, n_tp - 1)),
            dma((3, n_tp - 1)),
        ],
        compiler_params=pltpu.CompilerParams(
            collective_id=0, has_side_effects=True, vmem_limit_bytes=56 * 1024 * 1024
        ),
    )(
        tokens,
        lengths,
        keys,
        values,
        lambdas,
        head_gain,
        attn_gain,
        w_query,
        w_key,
        w_value,
        w_out,
        first_gain,
        first_gate,
        first_up,
        first_down,
        second_gain,
        second_gate,
        second_up,
        second_down,
        inv_freq,
    )


def solution(mesh):
    return jax.shard_map(
        functools.partial(local, mesh.shape["kv"], mesh.shape["tp"]),
        mesh=mesh,
        in_specs=(
            P(None, "kv"),
            P(),
            P(None, "kv", "tp", None),
            P(None, "kv", "tp", None),
            P("tp"),
            P(),
            P("kv"),
            P("kv", "tp"),
            P("kv", "tp"),
            P("kv", "tp"),
            P("tp", "kv"),
            P("kv"),
            P("kv", "tp"),
            P("kv", "tp"),
            P("tp", "kv"),
            P("kv"),
            P("kv", "tp"),
            P("kv", "tp"),
            P("tp", "kv"),
        ),
        out_specs=P(None, "kv"),
        check_vma=False,
    )
```

time: 45.8 us -> 39.9 us (0.87)
  Pallas kernels: 44.1 us -> 39.1 us
  local copies, waits for them, and re-layouts: 1.32 us -> 0.61 us
    pallas_call x1, Pallas kernels: 44.1 us -> 39.1 us  [local(): pl.pallas_call(functools.partial(kernel, n_kv, n_tp, cols * n_kv), out_sh...]
    unnamed x1, local copies, waits for them, and re-layouts: 1.32 us -> 0.61 us
where the time goes in v1:
time: 39.9 us; the launch traced here: 39.7 us
  Pallas kernels  39.1 us (98%)
  local copies, waits for them, and re-layouts  0.61 us (2%)
    pallas_call x1, Pallas kernels, local(): pl.pallas_call(functools.partial(kernel, n_kv, n_tp, cols * n_kv), out_sh...  39.1 us

profile of v1, /device:TPU:0, one launch (start us, length us, event | category | flops | bytes accessed | tf_op | source)
XLA Modules:
  0.0 39.7 jit_solution(7053860501081135201)
XLA Ops:
  0.0 39.1 %shard_map.190 = bf16[16,512]{1,0:T(8,128)(2,1)S(1)} custom-call(bf16[16,512]{1,0:T(8,128)(2,1)} %tokens_hbm.1, s32[16]{0:T(128)} %lengths_hbm.1, bf16[16,2048,128]{2,1,0:T(8,128)(2,1)} %bitcast.6, bf16[16,2048,128]{2,1,0:T(8,128)(2,1)} %bitcast.7, f32[2]{0:T(128)} %lambdas_hbm.1, bf16[128]{0:T(256)(128)(2,1)} %head_gain_hbm.1, bf16[512]{0:T(512)(128)(2,1)} %attn_gain_hbm.1, ...), custom_call_target="tpu_custom_call" | custom-call | tf_op jit(solution)/shard_map/pallas_call | solution.py:415
  39.1 0.6 %copy.22 = bf16[16,512]{1,0:T(8,128)(2,1)} copy(bf16[16,512]{1,0:T(8,128)(2,1)S(1)} %shard_map.190) | data formatting | bytes 32768
